TPU v7x, 256 devices: a whole 4x4x8 slice. The times are simulated.
256 devices in a mesh: fs: 32 (over z, x), tp: 8 (over y, core).
Axes of the slice: x: 4, y: 4, z: 8, core: 2. Of those that a mesh axis runs over, the one named last changes fastest.
Arguments:
- later_rows: bfloat16 [32768, 2048], P(('fs', 'tp')), may hold values from -6 to 6
- earlier_rows: bfloat16 [32768, 2048], P(('fs', 'tp')), may hold values from -6 to 6
- cotangent: bfloat16 [32768, 2048], P(('fs', 'tp')), may hold values from -24 to 24
- up_weight: bfloat16 [2048, 4096], P('fs', 'tp'), may hold values from -0.125 to 0.125
- down_weight: bfloat16 [2048, 4096], P('fs', 'tp'), may hold values from -0.09375 to 0.09375
- up_total: float32 [2048, 4096], P('fs', 'tp'), may hold values from -6 to 6
- down_total: float32 [2048, 4096], P('fs', 'tp'), may hold values from -6 to 6
Outputs:
- later_out: bfloat16 [32768, 2048], P(('fs', 'tp'))
- earlier_grad: bfloat16 [32768, 2048], P(('fs', 'tp'))
- up_updated: float32 [2048, 4096], P('fs', 'tp')
- down_updated: float32 [2048, 4096], P('fs', 'tp')
All inputs are finite; a program needn't handle non-finite values.
Results may differ from a plain program's by a relative error of at most 0.015.
Values may be sent and summed in bfloat16 or wider, within the bound.
No kernel may reach another device: no remote copies, remote signals or barrier semaphores. Data moves between devices by JAX's collectives and lax.ppermute only.
A program may use at most 128 MiB of HBM per device.

v0:
```python
import math
import jax
import jax.numpy as jnp
from jax import lax
from jax.sharding import Mesh
from jax.sharding import PartitionSpec as P

FS = ("fs_0", "fs_1")
FS_TP = ("fs_0", "fs_1", "tp")


def side_by_side(arrays, axis, dim, along):
    ends, at = ([], 0)
    for a in arrays[:-1]:
        at += a.shape[along]
        ends.append(at)
    both = jnp.concatenate(arrays, axis=along)
    return tuple(jnp.split(lax.all_gather(both, axis, axis=dim, tiled=True), ends, axis=along))


def in_blocks(x, dim, length):
    before, after = (x.shape[:dim], x.shape[dim + 1 :])
    return jnp.moveaxis(x.reshape(*before, length, -1, *after), dim, 0)


def sum_at_owner(x, axis, dim):
    length = lax.axis_size(axis)
    tiles = lax.all_to_all(in_blocks(x, dim, length), axis, 0, 0, tiled=True)
    return jnp.sum(tiles.astype(jnp.float32), axis=0)


def sum_by_axis(terms, axes):
    subtotal = terms.astype(jnp.bfloat16)
    for axis in axes:
        subtotal = lax.psum_scatter(subtotal, axis, scatter_dimension=0, tiled=True)
    return subtotal.astype(jnp.float32)


def contract_last(left, right):
    return lax.dot_general(
        left, right, (((1,), (1,)), ((), ())), preferred_element_type=jnp.float32
    )


def body(later_rows, earlier_rows, cotangent, up_weight, down_weight, up_total, down_total):
    rows_dev = later_rows.shape[0]
    total_rows = rows_dev * lax.axis_size(FS) * lax.axis_size("tp")
    factor = 1.0 / math.sqrt(total_rows)
    up_full, down_full = side_by_side((up_weight, down_weight), FS, 0, 1)

    def fetch():
        return (up_full, down_full)

    def to_owner(term):
        return sum_at_owner(term.astype(jnp.bfloat16), "tp", 0)

    def grad_owner(group, right):
        return sum_by_axis(
            lax.dot_general(
                group, right, (((0,), (0,)), ((), ())), preferred_element_type=jnp.float32
            ),
            FS,
        )

    up_whole, down_whole = fetch()
    group = lax.all_gather(later_rows, "tp", axis=0, tiled=True)
    relu_part = jnp.maximum(jnp.dot(group, up_whole, preferred_element_type=jnp.float32), 0.0)
    hidden = (relu_part * relu_part).astype(jnp.bfloat16)
    partial_value = contract_last(hidden, down_whole)
    later_out = to_owner(partial_value).astype(jnp.bfloat16)
    up_whole, down_whole = fetch()
    saved_group, cot_group = side_by_side((earlier_rows, cotangent), "tp", 0, 1)
    relu_part = jnp.maximum(jnp.dot(saved_group, up_whole, preferred_element_type=jnp.float32), 0.0)
    hidden = (relu_part * relu_part).astype(jnp.bfloat16)
    hidden_grad = jnp.dot(cot_group, down_whole, preferred_element_type=jnp.float32)
    pre_grad = (2.0 * relu_part * hidden_grad).astype(jnp.bfloat16)
    input_partial = contract_last(pre_grad, up_whole)
    earlier_grad = to_owner(input_partial).astype(jnp.bfloat16)
    down_updated = down_total + grad_owner(cot_group, hidden) * factor
    up_updated = up_total + grad_owner(saved_group, pre_grad) * factor
    earlier_grad, up_updated, down_updated = (earlier_grad, up_updated, down_updated)
    return (later_out, earlier_grad, up_updated, down_updated)


def solution(mesh):
    finer = Mesh(mesh.devices.reshape(8, 4, mesh.shape["tp"]), ("fs_0", "fs_1", "tp"))
    placed = (
        P(FS_TP, None),
        P(FS_TP, None),
        P(FS_TP, None),
        P(FS, "tp"),
        P(FS, "tp"),
        P(FS, "tp"),
        P(FS, "tp"),
    )
    return jax.shard_map(
        body,
        mesh=finer,
        in_specs=placed,
        out_specs=(P(FS_TP, None), P(FS_TP, None), P(FS, "tp"), P(FS, "tp")),
        check_vma=False,
    )
```

profile of v0, /device:TPU:8, one launch (start us, length us, event | category | flops | bytes accessed | tf_op | source)
XLA Modules:
  0.0 330.6 jit_solution(11753121503092980763)
XLA Ops:
  7.2 0.0 all-gather.4.cloned.1.call-start
  7.2 1.5 pad_maximum_fusion.1
  8.7 0.0 all-gather.4.cloned.1.call-update
  8.8 0.0 all-gather.8.cloned.1.call-start
  8.8 2.3 pad_maximum_fusion
  11.1 0.0 all-gather.8.cloned.1.call-update
  11.1 0.0 all-gather.6.cloned.1.call-start
  11.2 0.7 all-gather.6.cloned.1.call-update
  11.9 0.0 reduce-scatter.9.cloned.1.call-start
  11.9 83.9 %all-gather.4.cloned.1.call-done = bf16[2048,1024]{1,0:T(8,128)(2,1)} async-done(((bf16[64,1024]{1,0:T(8,128)(2,1)}), bf16[2048,1024]{1,0:T(8,128)(2,1)}) %all-gather.4.cloned.1.call-update) | async-done | bytes 4194320 | tf_op jit(solution)/shard_map/all_gather | solution.py:18
  95.8 50.1 %all-gather.8.cloned.1.call-done = bf16[1024,4096]{1,0:T(8,128)(2,1)} async-done(((bf16[128,4096]{1,0:T(8,128)(2,1)}), bf16[1024,4096]{1,0:T(8,128)(2,1)}) %all-gather.8.cloned.1.call-update) | async-done | bytes 8388624 | tf_op jit(solution)/shard_map/all_gather | solution.py:18
  145.9 0.0 copy-start.2
  145.9 5.3 %fusion.6 = f32[1024,512]{1,0:T(8,128)S(1)} fusion(bf16[1024,4096]{1,0:T(8,128)(2,1)} %all-gather.8.cloned.1.call-done, bf16[2048,1024]{1,0:T(8,128)(2,1)} %all-gather.4.cloned.1.call-done), kind=kOutput, calls=%fused_computation.8 | convolution fusion | flops 2147483648 | bytes 8388608 | tf_op jit(solution)/shard_map/dot_general | solution.py:73
  151.2 0.0 copy-done.2
  151.2 3.7 %fusion.11 = bf16[2048,512]{1,0:T(8,128)(2,1)} fusion(bf16[1024,4096]{1,0:T(8,128)(2,1)S(1)} %copy-done.2, f32[1024,512]{1,0:T(8,128)S(1)} %fusion.6), kind=kOutput, calls=%fused_computation.11 | convolution fusion | flops 2150105088 | bytes 8388608 | tf_op jit(solution)/shard_map/dot_general | solution.py:59
  154.9 0.0 reduce-scatter.9.cloned.1.call-update
  155.0 27.4 %all-gather.6.cloned.1.call-done = bf16[1024,2048]{1,0:T(8,128)(2,1)} async-done(((bf16[128,2048]{1,0:T(8,128)(2,1)}), bf16[1024,2048]{1,0:T(8,128)(2,1)}) %all-gather.6.cloned.1.call-update) | async-done | bytes 4194320 | tf_op jit(solution)/shard_map/all_gather | solution.py:66
  182.4 10.0 %convolution_convert_fusion.1 = bf16[1024,2048]{1,0:T(8,128)(2,1)} fusion(bf16[2048,1024]{1,0:T(8,128)(2,1)} %all-gather.4.cloned.1.call-done, bf16[1024,2048]{1,0:T(8,128)(2,1)} %all-gather.6.cloned.1.call-done), kind=kOutput, calls=%fused_computation.1 | convolution fusion | flops 4298637312 | bytes 12582912 | tf_op jit(solution)/shard_map/dot_general | solution.py:40
  192.4 6.0 %all-to-all-start = ((bf16[8,128,2048]{2,1,0:T(8,128)(2,1)}), bf16[8,128,2048]{2,1,0:T(8,128)(2,1)}, u32[]{:S(2)}, u32[]{:S(2)}) async-start(bf16[8,128,2048]{2,1,0:T(8,128)(2,1)} %bitcast.6), calls=%async_computation | async-start | bytes 8388608 | tf_op jit(solution)/shard_map/all_to_all | solution.py:28
  198.4 0.0 reduce-scatter.5.cloned.1.call-start
  198.4 5.2 %multiply_convert_fusion.1 = bf16[1024,512]{1,0:T(8,128)(2,1)S(1)} fusion(f32[1024,512]{1,0:T(8,128)S(1)} %fusion.6, bf16[2048,1024]{1,0:T(8,128)(2,1)} %all-gather.4.cloned.1.call-done, bf16[1024,4096]{1,0:T(8,128)(2,1)} %all-gather.8.cloned.1.call-done), kind=kOutput, calls=%fused_computation.13 | convolution fusion | flops 2149580800 | bytes 9437184 | tf_op jit(solution)/shard_map/dot_general | solution.py:75
  203.6 6.0 %fusion.8 = bf16[2048,512]{1,0:T(8,128)(2,1)} fusion(bf16[1024,512]{1,0:T(8,128)(2,1)S(1)} %multiply_convert_fusion.1, bf16[1024,4096]{1,0:T(8,128)(2,1)} %all-gather.8.cloned.1.call-done), kind=kOutput, calls=%fused_computation.10 | convolution fusion | flops 2148532224 | bytes 7340032 | tf_op jit(solution)/shard_map/dot_general | solution.py:59
  209.5 0.0 reduce-scatter.5.cloned.1.call-update
  209.6 5.9 %convolution_convert_fusion = bf16[1024,2048]{1,0:T(8,128)(2,1)} fusion(bf16[1024,512]{1,0:T(8,128)(2,1)S(1)} %multiply_convert_fusion.1, bf16[2048,1024]{1,0:T(8,128)(2,1)} %all-gather.4.cloned.1.call-done), kind=kOutput, calls=%fused_computation | convolution fusion | flops 2149580800 | bytes 7340032 | tf_op jit(solution)/shard_map/dot_general | solution.py:40
  215.5 31.2 %all-to-all-done = bf16[8,128,2048]{2,1,0:T(8,128)(2,1)} async-done(((bf16[8,128,2048]{2,1,0:T(8,128)(2,1)}), bf16[8,128,2048]{2,1,0:T(8,128)(2,1)}, u32[]{:S(2)}, u32[]{:S(2)}) %all-to-all-start) | async-done | bytes 4194336 | tf_op jit(solution)/shard_map/all_to_all | solution.py:28
  246.7 5.9 %all-to-all-start.1 = ((bf16[8,128,2048]{2,1,0:T(8,128)(2,1)}), bf16[8,128,2048]{2,1,0:T(8,128)(2,1)}, u32[]{:S(2)}, u32[]{:S(2)}) async-start(bf16[8,128,2048]{2,1,0:T(8,128)(2,1)} %bitcast.5), calls=%async_computation.1 | async-start | bytes 8388608 | tf_op jit(solution)/shard_map/all_to_all | solution.py:28
  252.6 0.0 reduce-scatter.11.cloned.1.call-start
  252.6 0.0 reduce-scatter.9.cloned.1.call-done
  252.6 0.6 reduce-scatter.11.cloned.1.call-update
  253.2 0.0 reduce-scatter.7.cloned.1.call-start
  253.2 18.8 %reduce-scatter.5.cloned.1.call-done = bf16[256,512]{1,0:T(8,128)(2,1)} async-done(((bf16[2048,512]{1,0:T(8,128)(2,1)}), bf16[256,512]{1,0:T(8,128)(2,1)}) %reduce-scatter.5.cloned.1.call-update) | async-done | bytes 262160 | tf_op jit(solution)/shard_map/reduce_scatter | solution.py:35
  272.0 0.0 reduce-scatter.7.cloned.1.call-update
  272.0 0.0 copy-start
  272.0 0.0 copy-start.1
  272.0 3.9 %reduce_sum.24 = bf16[128,2048]{1,0:T(8,128)(2,1)} reduce(bf16[8,128,2048]{2,1,0:T(8,128)(2,1)} %all-to-all-done, bf16[]{:T(256)} %constant.3.clone.1), dimensions={0}, to_apply=%region_0.0 | reduce | flops 1835008 | bytes 4718594 | tf_op jit(solution)/shard_map/reduce_sum | solution.py:29
  275.9 25.0 %all-to-all-done.1 = bf16[8,128,2048]{2,1,0:T(8,128)(2,1)} async-done(((bf16[8,128,2048]{2,1,0:T(8,128)(2,1)}), bf16[8,128,2048]{2,1,0:T(8,128)(2,1)}, u32[]{:S(2)}, u32[]{:S(2)}) %all-to-all-start.1) | async-done | bytes 4194336 | tf_op jit(solution)/shard_map/all_to_all | solution.py:28
  300.9 3.8 %reduce_sum.25 = bf16[128,2048]{1,0:T(8,128)(2,1)} reduce(bf16[8,128,2048]{2,1,0:T(8,128)(2,1)} %all-to-all-done.1, bf16[]{:T(256)} %constant.3.clone.1), dimensions={0}, to_apply=%region_1.0 | reduce | flops 1835008 | bytes 4718594 | tf_op jit(solution)/shard_map/reduce_sum | solution.py:29
  304.8 0.0 reduce-scatter.11.cloned.1.call-done
  304.8 0.0 copy-done
  304.8 1.5 multiply_add_fusion
  306.3 16.0 %reduce-scatter.7.cloned.1.call-done = bf16[64,512]{1,0:T(8,128)(2,1)} async-done(((bf16[256,512]{1,0:T(8,128)(2,1)}), bf16[64,512]{1,0:T(8,128)(2,1)}) %reduce-scatter.7.cloned.1.call-update) | async-done | bytes 65552 | tf_op jit(solution)/shard_map/reduce_scatter | solution.py:35
  322.3 0.0 copy-done.1
  322.3 1.5 multiply_add_fusion.1
Async XLA Ops:
  7.2 88.6 %all-gather.4.cloned.1.call-start = ((), (), s32[]{:S(2)}) async-start(), calls=%async_computation.6 | async-start | bytes 4325376 | tf_op jit(solution)/shard_map/all_gather | solution.py:18
  8.8 137.1 %all-gather.8.cloned.1.call-start = ((), (), s32[]{:S(2)}) async-start(), calls=%async_computation.8 | async-start | bytes 9437184 | tf_op jit(solution)/shard_map/all_gather | solution.py:18
  11.1 171.2 %all-gather.6.cloned.1.call-start = ((), (), s32[]{:S(2)}) async-start(), calls=%async_computation.7 | async-start | bytes 4718592 | tf_op jit(solution)/shard_map/all_gather | solution.py:66
  11.9 240.7 %reduce-scatter.9.cloned.1.call-start = ((), (), s32[]{:S(2)}) async-start(), calls=%async_computation.11 | async-start | bytes 2359296 | tf_op jit(solution)/shard_map/reduce_scatter | solution.py:35
  145.9 5.3 %copy-start.2 = (bf16[1024,4096]{1,0:T(8,128)(2,1)S(1)}, bf16[1024,4096]{1,0:T(8,128)(2,1)}, u32[]{:S(2)}) copy-start(bf16[1024,4096]{1,0:T(8,128)(2,1)} %all-gather.8.cloned.1.call-done) | copy-start | bytes 25165828
  192.4 54.3 %all-to-all-start = ((bf16[8,128,2048]{2,1,0:T(8,128)(2,1)}), bf16[8,128,2048]{2,1,0:T(8,128)(2,1)}, u32[]{:S(2)}, u32[]{:S(2)}) async-start(bf16[8,128,2048]{2,1,0:T(8,128)(2,1)} %bitcast.6), calls=%async_computation | async-start | bytes 8388608 | tf_op jit(solution)/shard_map/all_to_all | solution.py:28
  198.4 73.6 %reduce-scatter.5.cloned.1.call-start = ((), (), s32[]{:S(2)}) async-start(), calls=%async_computation.9 | async-start | bytes 2359296 | tf_op jit(solution)/shard_map/reduce_scatter | solution.py:35
  246.7 54.2 %all-to-all-start.1 = ((bf16[8,128,2048]{2,1,0:T(8,128)(2,1)}), bf16[8,128,2048]{2,1,0:T(8,128)(2,1)}, u32[]{:S(2)}, u32[]{:S(2)}) async-start(bf16[8,128,2048]{2,1,0:T(8,128)(2,1)} %bitcast.5), calls=%async_computation.1 | async-start | bytes 8388608 | tf_op jit(solution)/shard_map/all_to_all | solution.py:28
  252.6 52.2 %reduce-scatter.11.cloned.1.call-start = ((), (), s32[]{:S(2)}) async-start(), calls=%async_computation.12 | async-start | bytes 327680 | tf_op jit(solution)/shard_map/reduce_scatter | solution.py:35
  253.2 69.1 %reduce-scatter.7.cloned.1.call-start = ((), (), s32[]{:S(2)}) async-start(), calls=%async_computation.10 | async-start | bytes 327680 | tf_op jit(solution)/shard_map/reduce_scatter | solution.py:35
  272.0 32.8 %copy-start = (f32[64,512]{1,0:T(8,128)S(1)}, f32[64,512]{1,0:T(8,128)}, u32[]{:S(2)}) copy-start(f32[64,512]{1,0:T(8,128)} %param.13) | copy-start | bytes 393220
  272.0 50.3 %copy-start.1 = (f32[64,512]{1,0:T(8,128)S(1)}, f32[64,512]{1,0:T(8,128)}, u32[]{:S(2)}) copy-start(f32[64,512]{1,0:T(8,128)} %param.12) | copy-start | bytes 393220
Sparse Core Ops, SparseCore 0:
  11.1 84.6 all-gather.3
  97.6 48.1 all-gather.7
  147.8 34.5 all-gather.5
  184.8 43.4 reduce-scatter.8
  230.7 41.2 reduce-scatter.4
  274.3 22.1 reduce-scatter.10
  299.1 23.1 reduce-scatter.6
where the time goes:
time: 331 us
  waiting for transfers between devices  254 us (77%)
  matrix products  36.1 us (11%)
  other arithmetic  14.6 us (4%)
  between operations  14.2 us (4%)
  starting transfers between devices  12.1 us (4%)
    all_gather x2, waiting for transfers between devices, side_by_side(): lax.all_gather(both, axis, axis=dim, tiled=True)  134 us
    all_to_all x2, waiting for transfers between devices, sum_at_owner(): tiles = lax.all_to_all(in_blocks(x, dim, length), axis, 0, 0, tiled=True)  56.2 us
    reduce_scatter x4, waiting for transfers between devices, sum_by_axis(): subtotal = lax.psum_scatter(subtotal, axis, scatter_dimension=0, tiled=True)  34.8 us
    all_gather x1, waiting for transfers between devices, body(): group = lax.all_gather(later_rows, 'tp', axis=0, tiled=True)  27.4 us
    dot_general x2, matrix products, contract_last(): lax.dot_general(left, right, (((1,), (1,)), ((), ())), preferred_element_...  15.9 us
    all_to_all x2, starting transfers between devices, sum_at_owner(): tiles = lax.all_to_all(in_blocks(x, dim, length), axis, 0, 0, tiled=True)  11.9 us
    dot_general x2, matrix products, grad_owner(): lax.dot_general(group, right, (((0,), (0,)), ((), ())), preferred_element...  9.68 us
    reduce_sum x2, other arithmetic, sum_at_owner(): return jnp.sum(tiles.astype(jnp.float32), axis=0)  7.73 us
  transfers between devices with their start and end apart: 9, of which 7 were waited for; matrix products, arithmetic and copies ran while one was open for 14% of the time, Pallas kernels for 0%

commit v1 on v0

--- a/solution.py
+++ b/solution.py
@@ -63,7 +63,26 @@
         )
 
     up_whole, down_whole = fetch()
-    group = lax.all_gather(later_rows, "tp", axis=0, tiled=True)
+    val2 = lax.axis_size("tp")
+    new, newest, wide_out = (val2, lax.axis_index("tp"), later_rows.shape[0])
+    queue = [(j, (j + 1) % new) for j in range(new)]
+    all_blocks = [(j, (j - 1) % new) for j in range(new)]
+    group = jnp.zeros(
+        (*later_rows.shape[:0], new * wide_out, *later_rows.shape[0 + 1 :]), later_rows.dtype
+    )
+    group = lax.dynamic_update_slice_in_dim(group, later_rows, newest * wide_out, axis=0)
+    k_now = small = later_rows
+    value_now = new // 2
+    for dd in range(1, value_now + 1):
+        k_now = lax.ppermute(k_now, axis_name="tp", perm=queue)
+        group = lax.dynamic_update_slice_in_dim(
+            group, k_now, (newest - dd) % new * wide_out, axis=0
+        )
+        if dd < new - value_now:
+            small = lax.ppermute(small, "tp", all_blocks)
+            group = lax.dynamic_update_slice_in_dim(
+                group, small, (newest + dd) % new * wide_out, axis=0
+            )
     relu_part = jnp.maximum(jnp.dot(group, up_whole, preferred_element_type=jnp.float32), 0.0)
     hidden = (relu_part * relu_part).astype(jnp.bfloat16)
     partial_value = contract_last(hidden, down_whole)

time: 331 us -> 306 us (0.924)
  waiting for transfers between devices: 254 us -> 214 us
  local copies, waits for them, and re-layouts: 0.02 us -> 11.5 us
  starting transfers between devices: 12.1 us -> 17.6 us
    all_gather x1 -> x0, waiting for transfers between devices: 27.4 us -> none  [body(): group = lax.all_gather(later_rows, 'tp', axis=0, tiled=True)]
    all_gather x2, waiting for transfers between devices: 134 us -> 109 us  [side_by_side(): lax.all_gather(both, axis, axis=dim, tiled=True)]
    ppermute x0 -> x7, waiting for transfers between devices: none -> 14.6 us  [the longest x4 14.6 us: body(): k_now = lax.ppermute(k_now, axis_name='tp', perm=queue)]
    reduce_scatter x4, waiting for transfers between devices: 34.8 us -> 23.7 us  [sum_by_axis(): subtotal = lax.psum_scatter(subtotal, axis, scatter_dimension=0, tiled=True)]
    all_to_all x2, waiting for transfers between devices: 56.2 us -> 66.7 us  [sum_at_owner(): tiles = lax.all_to_all(in_blocks(x, dim, length), axis, 0, 0, tiled=True)]
    dynamic_update_slice x0 -> x8, local copies, waits for them, and re-layouts: none -> 6.84 us  [the longest x4 3.44 us: body(): lax.dynamic_update_slice_in_dim(group, k_now, (newest - dd) % new * wide_...]
    ppermute x0 -> x7, starting transfers between devices: none -> 5.54 us  [the longest x3 5.52 us: body(): small = lax.ppermute(small, 'tp', all_blocks)]
  transfers between devices with their start and end apart: 9 -> 15, of which waited for: 7 -> 9; matrix products, arithmetic and copies ran while one was open for 14% -> 18% of each run, Pallas kernels for 0% -> 0%
where the time goes in v1:
time: 306 us; the launch traced here: 305 us
  waiting for transfers between devices  214 us (70%)
  matrix products  33.2 us (11%)
  starting transfers between devices  17.6 us (6%)
  other arithmetic  14.6 us (5%)
  between operations  14.2 us (5%)
  local copies, waits for them, and re-layouts  11.5 us (4%)
    all_gather x2, waiting for transfers between devices, side_by_side(): lax.all_gather(both, axis, axis=dim, tiled=True)  109 us
    all_to_all x2, waiting for transfers between devices, sum_at_owner(): tiles = lax.all_to_all(in_blocks(x, dim, length), axis, 0, 0, tiled=True)  66.7 us
    reduce_scatter x4, waiting for transfers between devices, sum_by_axis(): subtotal = lax.psum_scatter(subtotal, axis, scatter_dimension=0, tiled=True)  23.7 us
    dot_general x2, matrix products, contract_last(): lax.dot_general(left, right, (((1,), (1,)), ((), ())), preferred_element_...  15.8 us
    ppermute x4, waiting for transfers between devices, body(): k_now = lax.ppermute(k_now, axis_name='tp', perm=queue)  14.6 us
    all_to_all x2, starting transfers between devices, sum_at_owner(): tiles = lax.all_to_all(in_blocks(x, dim, length), axis, 0, 0, tiled=True)  11.9 us
    dot_general x2, matrix products, grad_owner(): lax.dot_general(group, right, (((0,), (0,)), ((), ())), preferred_element...  9.77 us
    reduce_sum x2, other arithmetic, sum_at_owner(): return jnp.sum(tiles.astype(jnp.float32), axis=0)  7.73 us
  transfers between devices with their start and end apart: 15, of which 9 were waited for; matrix products, arithmetic and copies ran while one was open for 18% of the time, Pallas kernels for 0%

profile of v1, /device:TPU:8, one launch (start us, length us, event | category | flops | bytes accessed | tf_op | source)
XLA Modules:
  0.0 305.4 jit_solution(14399257976602891786)
XLA Ops:
  7.2 0.0 all-gather.3.cloned.1.call-start
  7.2 1.6 pad_maximum_fusion.1
  8.8 0.0 all-gather.3.cloned.1.call-update
  8.8 0.0 all-gather.5.cloned.1.call-start
  8.9 2.3 pad_maximum_fusion
  11.2 0.0 all-gather.5.cloned.1.call-update
  11.2 0.0 reduce-scatter.5.cloned.1.call-start
  11.2 0.0 collective-permute-start
  11.3 1.7 collective-permute-start.1
  13.0 7.1 %collective-permute-done = bf16[128,2048]{1,0:T(8,128)(2,1)S(1)} collective-permute-done((bf16[128,2048]{1,0:T(8,128)(2,1)}, bf16[128,2048]{1,0:T(8,128)(2,1)S(1)}, u32[]{:S(2)}, u32[]{:S(2)}) %collective-permute-start) | collective-permute-done | bytes 524320 | tf_op jit(solution)/shard_map/ppermute | solution.py:77
  20.1 2.0 collective-permute-start.3
  22.1 2.5 broadcast_in_dim.3
  24.6 0.8 constant_dynamic-update-slice_fusion.7
  25.4 3.3 %collective-permute-done.2 = bf16[128,2048]{1,0:T(8,128)(2,1)S(1)} collective-permute-done((bf16[128,2048]{1,0:T(8,128)(2,1)S(1)}, bf16[128,2048]{1,0:T(8,128)(2,1)S(1)}, u32[]{:S(2)}, u32[]{:S(2)}) %collective-permute-start.2) | collective-permute-done | bytes 524320 | tf_op jit(solution)/shard_map/ppermute | solution.py:77
  28.7 0.9 constant_dynamic-update-slice_fusion.6
  29.6 0.9 constant_dynamic-update-slice_fusion.5
  30.4 1.8 collective-permute-start.5
  32.2 0.9 constant_dynamic-update-slice_fusion.4
  33.0 4.2 %collective-permute-done.4 = bf16[128,2048]{1,0:T(8,128)(2,1)S(1)} collective-permute-done((bf16[128,2048]{1,0:T(8,128)(2,1)S(1)}, bf16[128,2048]{1,0:T(8,128)(2,1)S(1)}, u32[]{:S(2)}, u32[]{:S(2)}) %collective-permute-start.4) | collective-permute-done | bytes 524320 | tf_op jit(solution)/shard_map/ppermute | solution.py:77
  37.3 58.6 %all-gather.3.cloned.1.call-done = bf16[2048,1024]{1,0:T(8,128)(2,1)} async-done(((bf16[64,1024]{1,0:T(8,128)(2,1)}), bf16[2048,1024]{1,0:T(8,128)(2,1)}) %all-gather.3.cloned.1.call-update) | async-done | bytes 4194320 | tf_op jit(solution)/shard_map/all_gather | solution.py:18
  95.9 50.1 %all-gather.5.cloned.1.call-done = bf16[1024,4096]{1,0:T(8,128)(2,1)} async-done(((bf16[128,4096]{1,0:T(8,128)(2,1)}), bf16[1024,4096]{1,0:T(8,128)(2,1)}) %all-gather.5.cloned.1.call-update) | async-done | bytes 8388624 | tf_op jit(solution)/shard_map/all_gather | solution.py:18
  146.0 5.3 %fusion.6 = f32[1024,512]{1,0:T(8,128)S(1)} fusion(bf16[1024,4096]{1,0:T(8,128)(2,1)} %all-gather.5.cloned.1.call-done, bf16[2048,1024]{1,0:T(8,128)(2,1)} %all-gather.3.cloned.1.call-done), kind=kOutput, calls=%fused_computation.8 | convolution fusion | flops 2147483648 | bytes 8388608 | tf_op jit(solution)/shard_map/dot_general | solution.py:92
  151.3 1.1 copy-done.4
  152.4 2.3 multiply_convert_fusion.1
  154.8 1.1 copy-done.7
  155.8 3.7 %fusion.8 = bf16[2048,512]{1,0:T(8,128)(2,1)} fusion(bf16[1024,512]{1,0:T(8,128)(2,1)S(1)} %multiply_convert_fusion.1, bf16[1024,4096]{1,0:T(8,128)(2,1)S(1)} %copy-done.3), kind=kOutput, calls=%fused_computation.10 | convolution fusion | flops 2148532224 | bytes 7340032 | tf_op jit(solution)/shard_map/dot_general | solution.py:59
  159.6 0.0 reduce-scatter.5.cloned.1.call-update
  159.6 0.9 constant_dynamic-update-slice_fusion.3
  160.4 0.8 constant_dynamic-update-slice_fusion.2
  161.3 0.9 constant_dynamic-update-slice_fusion.1
  162.1 0.8 constant_dynamic-update-slice_fusion
  163.0 9.9 %convolution_convert_fusion.1 = bf16[1024,2048]{1,0:T(8,128)(2,1)} fusion(bf16[2048,1024]{1,0:T(8,128)(2,1)} %all-gather.3.cloned.1.call-done, bf16[1024,2048]{1,0:T(8,128)(2,1)} %constant_dynamic-update-slice_fusion), kind=kOutput, calls=%fused_computation.1 | convolution fusion | flops 4298637312 | bytes 12582912 | tf_op jit(solution)/shard_map/dot_general | solution.py:40
  172.9 6.0 %all-to-all-start = ((bf16[8,128,2048]{2,1,0:T(8,128)(2,1)}), bf16[8,128,2048]{2,1,0:T(8,128)(2,1)}, u32[]{:S(2)}, u32[]{:S(2)}) async-start(bf16[8,128,2048]{2,1,0:T(8,128)(2,1)} %bitcast.6), calls=%async_computation | async-start | bytes 8388608 | tf_op jit(solution)/shard_map/all_to_all | solution.py:28
  178.9 6.0 %fusion.11 = bf16[2048,512]{1,0:T(8,128)(2,1)} fusion(bf16[1024,4096]{1,0:T(8,128)(2,1)} %all-gather.5.cloned.1.call-done, f32[1024,512]{1,0:T(8,128)S(1)} %copy-done.6), kind=kOutput, calls=%fused_computation.11 | convolution fusion | flops 2150105088 | bytes 8388608 | tf_op jit(solution)/shard_map/dot_general | solution.py:59
  184.9 0.0 reduce-scatter.9.cloned.1.call-update
  184.9 5.9 %convolution_convert_fusion = bf16[1024,2048]{1,0:T(8,128)(2,1)} fusion(bf16[1024,512]{1,0:T(8,128)(2,1)S(1)} %copy-done.8, bf16[2048,1024]{1,0:T(8,128)(2,1)} %all-gather.3.cloned.1.call-done), kind=kOutput, calls=%fused_computation | convolution fusion | flops 2149580800 | bytes 7340032 | tf_op jit(solution)/shard_map/dot_general | solution.py:40
  190.9 36.3 %all-to-all-done = bf16[8,128,2048]{2,1,0:T(8,128)(2,1)} async-done(((bf16[8,128,2048]{2,1,0:T(8,128)(2,1)}), bf16[8,128,2048]{2,1,0:T(8,128)(2,1)}, u32[]{:S(2)}, u32[]{:S(2)}) %all-to-all-start) | async-done | bytes 4194336 | tf_op jit(solution)/shard_map/all_to_all | solution.py:28
  227.2 5.9 %all-to-all-start.1 = ((bf16[8,128,2048]{2,1,0:T(8,128)(2,1)}), bf16[8,128,2048]{2,1,0:T(8,128)(2,1)}, u32[]{:S(2)}, u32[]{:S(2)}) async-start(bf16[8,128,2048]{2,1,0:T(8,128)(2,1)} %bitcast.5), calls=%async_computation.1 | async-start | bytes 8388608 | tf_op jit(solution)/shard_map/all_to_all | solution.py:28
  233.1 0.6 reduce-scatter.7.cloned.1.call-update
  233.6 0.0 reduce-scatter.11.cloned.1.call-start
  233.7 13.4 %reduce-scatter.9.cloned.1.call-done = bf16[256,512]{1,0:T(8,128)(2,1)} async-done(((bf16[2048,512]{1,0:T(8,128)(2,1)}), bf16[256,512]{1,0:T(8,128)(2,1)}) %reduce-scatter.9.cloned.1.call-update) | async-done | bytes 262160 | tf_op jit(solution)/shard_map/reduce_scatter | solution.py:35
  247.1 0.0 reduce-scatter.11.cloned.1.call-update
  247.1 3.9 %reduce_sum.24 = bf16[128,2048]{1,0:T(8,128)(2,1)} reduce(bf16[8,128,2048]{2,1,0:T(8,128)(2,1)} %all-to-all-done, bf16[]{:T(256)} %constant.55.clone.1), dimensions={0}, to_apply=%region_0.1 | reduce | flops 1835008 | bytes 4718594 | tf_op jit(solution)/shard_map/reduce_sum | solution.py:29
  251.0 30.4 %all-to-all-done.1 = bf16[8,128,2048]{2,1,0:T(8,128)(2,1)} async-done(((bf16[8,128,2048]{2,1,0:T(8,128)(2,1)}), bf16[8,128,2048]{2,1,0:T(8,128)(2,1)}, u32[]{:S(2)}, u32[]{:S(2)}) %all-to-all-start.1) | async-done | bytes 4194336 | tf_op jit(solution)/shard_map/all_to_all | solution.py:28
  281.4 3.8 %reduce_sum.25 = bf16[128,2048]{1,0:T(8,128)(2,1)} reduce(bf16[8,128,2048]{2,1,0:T(8,128)(2,1)} %all-to-all-done.1, bf16[]{:T(256)} %constant.55.clone.1), dimensions={0}, to_apply=%region_1.2 | reduce | flops 1835008 | bytes 4718594 | tf_op jit(solution)/shard_map/reduce_sum | solution.py:29
  285.2 1.5 multiply_add_fusion.1
  286.7 10.3 %reduce-scatter.11.cloned.1.call-done = bf16[64,512]{1,0:T(8,128)(2,1)} async-done(((bf16[256,512]{1,0:T(8,128)(2,1)}), bf16[64,512]{1,0:T(8,128)(2,1)}) %reduce-scatter.11.cloned.1.call-update) | async-done | bytes 65552 | tf_op jit(solution)/shard_map/reduce_scatter | solution.py:35
  297.0 1.5 multiply_add_fusion
  (27 shorter events, 0.1 us)
Async XLA Ops:
  7.2 17.4 %copy-start = (bf16[128,2048]{1,0:T(8,128)(2,1)S(1)}, bf16[128,2048]{1,0:T(8,128)(2,1)}, u32[]{:S(2)}) copy-start(bf16[128,2048]{1,0:T(8,128)(2,1)} %param.7) | copy-start | bytes 1572868
  7.2 88.7 %all-gather.3.cloned.1.call-start = ((), (), s32[]{:S(2)}) async-start(), calls=%async_computation.6 | async-start | bytes 4325376 | tf_op jit(solution)/shard_map/all_gather | solution.py:18
  8.8 137.1 %all-gather.5.cloned.1.call-start = ((), (), s32[]{:S(2)}) async-start(), calls=%async_computation.7 | async-start | bytes 9437184 | tf_op jit(solution)/shard_map/all_gather | solution.py:18
  11.2 221.9 %reduce-scatter.5.cloned.1.call-start = ((), (), s32[]{:S(2)}) async-start(), calls=%async_computation.8 | async-start | bytes 2359296 | tf_op jit(solution)/shard_map/reduce_scatter | solution.py:35
  11.2 8.8 %collective-permute-start = (bf16[128,2048]{1,0:T(8,128)(2,1)}, bf16[128,2048]{1,0:T(8,128)(2,1)S(1)}, u32[]{:S(2)}, u32[]{:S(2)}) collective-permute-start(bf16[128,2048]{1,0:T(8,128)(2,1)} %param.7), channel_id=1, source_target_pairs={{0,1},{1,2},{2,3},{3,4},{4,5},{5,6},{6,7},{7,0},{8,9},{9,10},{10,1... | collective-permute-start | bytes 1572872 | tf_op jit(solution)/shard_map/ppermute | solution.py:77
  11.3 8.8 %collective-permute-start.1 = (bf16[128,2048]{1,0:T(8,128)(2,1)}, bf16[128,2048]{1,0:T(8,128)(2,1)S(1)}, u32[]{:S(2)}, u32[]{:S(2)}) collective-permute-start(bf16[128,2048]{1,0:T(8,128)(2,1)} %param.7), channel_id=1, source_target_pairs={{0,7},{1,0},{2,1},{3,2},{4,3},{5,4},{6,5},{7,6},{8,15},{9,8},{10,9... | collective-permute-start | bytes 1572872 | tf_op jit(solution)/shard_map/ppermute | solution.py:82
  20.1 8.6 %collective-permute-start.2 = (bf16[128,2048]{1,0:T(8,128)(2,1)S(1)}, bf16[128,2048]{1,0:T(8,128)(2,1)S(1)}, u32[]{:S(2)}, u32[]{:S(2)}) collective-permute-start(bf16[128,2048]{1,0:T(8,128)(2,1)S(1)} %collective-permute-done), channel_id=1, source_target_pairs={{0,1},{1,2},{2,3},{3,4},{4,5},{5,6},{6,7},{7,0},{8,9},{9,10},{10,1... | collective-permute-start | bytes 1572872 | tf_op jit(solution)/shard_map/ppermute | solution.py:77
  20.1 10.3 %collective-permute-start.3 = (bf16[128,2048]{1,0:T(8,128)(2,1)S(1)}, bf16[128,2048]{1,0:T(8,128)(2,1)S(1)}, u32[]{:S(2)}, u32[]{:S(2)}) collective-permute-start(bf16[128,2048]{1,0:T(8,128)(2,1)S(1)} %collective-permute-done.1), channel_id=1, source_target_pairs={{0,7},{1,0},{2,1},{3,2},{4,3},{5,4},{6,5},{7,6},{8,15},{9,8},{10,9... | collective-permute-start | bytes 1572872 | tf_op jit(solution)/shard_map/ppermute | solution.py:82
  28.7 8.6 %collective-permute-start.4 = (bf16[128,2048]{1,0:T(8,128)(2,1)S(1)}, bf16[128,2048]{1,0:T(8,128)(2,1)S(1)}, u32[]{:S(2)}, u32[]{:S(2)}) collective-permute-start(bf16[128,2048]{1,0:T(8,128)(2,1)S(1)} %collective-permute-done.2), channel_id=1, source_target_pairs={{0,1},{1,2},{2,3},{3,4},{4,5},{5,6},{6,7},{7,0},{8,9},{9,10},{10,1... | collective-permute-start | bytes 1572872 | tf_op jit(solution)/shard_map/ppermute | solution.py:77
  30.4 130.9 %collective-permute-start.5 = (bf16[128,2048]{1,0:T(8,128)(2,1)S(1)}, bf16[128,2048]{1,0:T(8,128)(2,1)S(1)}, u32[]{:S(2)}, u32[]{:S(2)}) collective-permute-start(bf16[128,2048]{1,0:T(8,128)(2,1)S(1)} %collective-permute-done.3), channel_id=1, source_target_pairs={{0,7},{1,0},{2,1},{3,2},{4,3},{5,4},{6,5},{7,6},{8,15},{9,8},{10,9... | collective-permute-start | bytes 1572872 | tf_op jit(solution)/shard_map/ppermute | solution.py:82
  37.3 124.9 %collective-permute-start.6 = (bf16[128,2048]{1,0:T(8,128)(2,1)S(1)}, bf16[128,2048]{1,0:T(8,128)(2,1)S(1)}, u32[]{:S(2)}, u32[]{:S(2)}) collective-permute-start(bf16[128,2048]{1,0:T(8,128)(2,1)S(1)} %collective-permute-done.4), channel_id=1, source_target_pairs={{0,1},{1,2},{2,3},{3,4},{4,5},{5,6},{6,7},{7,0},{8,9},{9,10},{10,1... | collective-permute-start | bytes 1572872 | tf_op jit(solution)/shard_map/ppermute | solution.py:77
  146.0 5.3 %copy-start.3 = (bf16[1024,4096]{1,0:T(8,128)(2,1)S(1)}, bf16[1024,4096]{1,0:T(8,128)(2,1)}, u32[]{:S(2)}) copy-start(bf16[1024,4096]{1,0:T(8,128)(2,1)} %all-gather.5.cloned.1.call-done) | copy-start | bytes 25165828
  146.0 6.4 %copy-start.4 = (bf16[2048,1024]{1,0:T(8,128)(2,1)S(1)}, bf16[2048,1024]{1,0:T(8,128)(2,1)}, u32[]{:S(2)}) copy-start(bf16[2048,1024]{1,0:T(8,128)(2,1)} %all-gather.3.cloned.1.call-done) | copy-start | bytes 12582916
  152.4 2.3 copy-start.5
  154.8 1.1 copy-start.7
  172.9 6.0 %copy-start.6 = (f32[1024,512]{1,0:T(8,128)S(1)}, f32[1024,512]{1,0:T(8,128)}, u32[]{:S(2)}) copy-start(f32[1024,512]{1,0:T(8,128)} %copy-done.5) | copy-start | bytes 6291460
  172.9 54.3 %all-to-all-start = ((bf16[8,128,2048]{2,1,0:T(8,128)(2,1)}), bf16[8,128,2048]{2,1,0:T(8,128)(2,1)}, u32[]{:S(2)}, u32[]{:S(2)}) async-start(bf16[8,128,2048]{2,1,0:T(8,128)(2,1)} %bitcast.6), calls=%async_computation | async-start | bytes 8388608 | tf_op jit(solution)/shard_map/all_to_all | solution.py:28
  178.8 6.1 %copy-start.8 = (bf16[1024,512]{1,0:T(8,128)(2,1)S(1)}, bf16[1024,512]{1,0:T(8,128)(2,1)}, u32[]{:S(2)}) copy-start(bf16[1024,512]{1,0:T(8,128)(2,1)} %copy-done.7) | copy-start | bytes 3145732
  178.8 68.2 %reduce-scatter.9.cloned.1.call-start = ((), (), s32[]{:S(2)}) async-start(), calls=%async_computation.10 | async-start | bytes 2359296 | tf_op jit(solution)/shard_map/reduce_scatter | solution.py:35
  227.2 54.2 %all-to-all-start.1 = ((bf16[8,128,2048]{2,1,0:T(8,128)(2,1)}), bf16[8,128,2048]{2,1,0:T(8,128)(2,1)}, u32[]{:S(2)}, u32[]{:S(2)}) async-start(bf16[8,128,2048]{2,1,0:T(8,128)(2,1)} %bitcast.5), calls=%async_computation.1 | async-start | bytes 8388608 | tf_op jit(solution)/shard_map/all_to_all | solution.py:28
  233.1 52.2 %reduce-scatter.7.cloned.1.call-start = ((), (), s32[]{:S(2)}) async-start(), calls=%async_computation.9 | async-start | bytes 327680 | tf_op jit(solution)/shard_map/reduce_scatter | solution.py:35
  233.6 63.4 %reduce-scatter.11.cloned.1.call-start = ((), (), s32[]{:S(2)}) async-start(), calls=%async_computation.11 | async-start | bytes 327680 | tf_op jit(solution)/shard_map/reduce_scatter | solution.py:35
  247.1 38.1 %copy-start.1 = (f32[64,512]{1,0:T(8,128)S(1)}, f32[64,512]{1,0:T(8,128)}, u32[]{:S(2)}) copy-start(f32[64,512]{1,0:T(8,128)} %param.12) | copy-start | bytes 393220
  247.1 49.9 %copy-start.2 = (f32[64,512]{1,0:T(8,128)S(1)}, f32[64,512]{1,0:T(8,128)}, u32[]{:S(2)}) copy-start(f32[64,512]{1,0:T(8,128)} %param.13) | copy-start | bytes 393220
Sparse Core Ops, SparseCore 0:
  11.1 84.6 all-gather.2
  97.7 48.1 all-gather.4
  159.7 43.8 reduce-scatter.4
  206.0 41.0 reduce-scatter.8
  249.4 22.0 reduce-scatter.6
  273.9 23.1 reduce-scatter.10
